TPU v7x, 32 devices: a whole 2x2x4 slice. The times are simulated.
32 devices in a mesh: sp: 8 (over z, y), dp: 4 (over x, core).
Axes of the slice: x: 2, y: 2, z: 4, core: 2. Of those that a mesh axis runs over, the one named last changes fastest.
Arguments:
- queries: bfloat16 [4, 1024, 2048], P('dp', 'sp'), may hold values from -40 to 40
- keys: bfloat16 [4, 1024, 512], P('dp', 'sp'), may hold values from -8 to 8
- values: bfloat16 [4, 1024, 512], P('dp', 'sp'), may hold values from -6 to 6
- lambdas: float32 [16], replicated, may hold values from 0.3 to 0.8
- value_gain: float32 [128], replicated, may hold values from 0.1 to 1.9
- out_weight: bfloat16 [2048, 4096], P(None, ('sp', 'dp')), may hold values from -0.125 to 0.125
Outputs:
- mixed: bfloat16 [4, 1024, 4096], P('dp', 'sp')
All inputs are finite; a program needn't handle non-finite values.
Results may differ from a plain program's by a relative error of at most 0.0087.
Values may be sent and summed in bfloat16 or wider, within the bound.
A program may use at most 128 MiB of HBM per device.

v0:
```python
import functools

import jax
import jax.numpy as jnp
from jax import lax
from jax.experimental import pallas as pl
from jax.experimental.pallas import tpu as pltpu
from jax.sharding import PartitionSpec as P

HEADS = 16
KV_HEADS = 4
HEAD_DIM = 64
VALUE_DIM = 128
GROUP = HEADS // KV_HEADS

rope_base = 500000.0
output_scale = 0.8
norm_eps = 1e-05
MESH = pl.DeviceIdType.MESH


def tables(positions):
    freqs = rope_base ** (-jnp.arange(0, HEAD_DIM, 2, dtype=jnp.float32) / HEAD_DIM)
    angles = positions[:, None] * freqs[None, :]
    cosine, sine = jnp.cos(angles), jnp.sin(angles)
    return jnp.concatenate([cosine] * 4, -1), jnp.concatenate([-sine, sine, -sine, sine], -1)


def turn(block, cosine, sine):
    half = HEAD_DIM // 2
    lane = lax.broadcasted_iota(jnp.int32, block.shape, 1)
    other = jnp.where(
        lane % HEAD_DIM < half,
        pltpu.roll(block, block.shape[1] - half, 1),
        pltpu.roll(block, half, 1),
    )
    return block * cosine + other * sine


def send(src, dst, send_sem, recv_sem, axis, index):
    return pltpu.make_async_remote_copy(
        src_ref=src,
        dst_ref=dst,
        send_sem=send_sem,
        recv_sem=recv_sem,
        device_id={axis: index},
        device_id_type=MESH,
    )


def layer_kernel(
    n,
    count,
    lam_ref,
    q_ref,
    k_ref,
    v_ref,
    cos_ref,
    sin_ref,
    gain_ref,
    w_ref,
    out_ref,
    kv_own,
    kv_all,
    w_all,
    heads_all,
    built,
    own_sem,
    kv_send,
    kv_recv,
    w_send,
    w_recv,
    x_send,
    x_recv,
    mate_send,
    mate_recv,
    out_send,
    out_recv,
):
    bf16 = jnp.bfloat16
    d = lax.axis_index("dp")
    me = lax.axis_index("sp")
    half = count // 2
    tall = n // half
    steps = n // 2
    width = 2 * HEAD_DIM
    rows = q_ref.shape[0]
    seqlen = n * rows

    def flip(column, place):
        return place + column % 2 * (tall - 1 - 2 * place)

    pos = me % half * tall + flip(me % half, me // half)

    def at(place):
        place = (place + 2 * n) % n
        column = place // tall
        return flip(column, place % tall) * half + column

    ahead, behind = at(pos + 1), at(pos - 1)
    x, core = d // 2, d % 2
    mate = x * 2 + 1 - core

    def peer(k):
        return (x + k) % half * 2 + core

    barrier = pltpu.get_barrier_semaphore()
    for other in (ahead, behind):
        pl.semaphore_signal(barrier, inc=1, device_id={"sp": other}, device_id_type=MESH)
    for k in range(1, count):
        pl.semaphore_signal(barrier, inc=1, device_id={"dp": (d + k) % count}, device_id_type=MESH)
    for g in range(KV_HEADS):
        cols = slice(g * width, (g + 1) * width)
        key = turn(k_ref[:, cols].astype(jnp.float32), cos_ref[...], sin_ref[...])
        kv_own[:, cols] = key.astype(bf16)
    kv_own[:, KV_HEADS * width :] = v_ref[...]
    pl.semaphore_wait(barrier, count + 1)

    def ring_step(own, held, sends, recvs, t, p):
        cut = held.shape[1] // 2
        part = pl.ds(p * cut, cut)
        copies = []
        for way in range(2) if t < steps else (p,):
            slot = at(pos - (t - 1)) if way == 0 else at(pos + (t - 1))
            dst = held.at[slot].at[part]
            copies.append(
                send(
                    own.at[part] if t == 1 else dst,
                    dst,
                    sends.at[way, t - 1, p],
                    recvs.at[way, t - 1, p],
                    "sp",
                    behind if way else ahead,
                )
            )
            copies[-1].start()
        return copies

    kv_copies, w_copies = {}, {}

    def kv_step(t, p):
        kv_copies[t, p] = ring_step(kv_own, kv_all, kv_send, kv_recv, t, p)

    def w_step(t, p):
        w_copies[t, p] = ring_step(w_ref, w_all, w_send, w_recv, t, p)

    kv_step(1, 0)
    kv_step(1, 1)
    local = pltpu.make_async_copy(kv_own, kv_all.at[me], own_sem)
    local.start()
    for t in range(1, steps + 1):
        for p in range(2):
            for copy in kv_copies[t, p]:
                copy.wait_recv()
            if t < steps:
                kv_step(t + 1, p)
        if t == steps - 1:
            w_step(1, 0)
            w_step(1, 1)
    local.wait()

    def w_relay(t, p):
        for copy in w_copies[t, p]:
            copy.wait_recv()
        if t < steps:
            w_step(t + 1, p)

    allowed = lax.broadcasted_iota(jnp.int32, (rows, seqlen), 1) <= (
        me * rows + lax.broadcasted_iota(jnp.int32, (rows, seqlen), 0)
    )
    lane = lax.broadcasted_iota(jnp.int32, (rows, width), 1)

    def span(g):
        return pl.ds(pl.multiple_of(g * GROUP * VALUE_DIM, GROUP * VALUE_DIM), GROUP * VALUE_DIM)

    def sends_of(g):
        part = heads_all.at[d, :, span(g)]
        result = [send(part, part, x_send.at[0, g], x_recv.at[0, g], "dp", mate)]
        for k in range(1, half):
            result.append(send(part, part, x_send.at[k, g], x_recv.at[k, g], "dp", peer(k)))
        return result

    def one_group(g, carry):
        key = kv_all[:, :, pl.ds(pl.multiple_of(g * width, width), width)]
        key = key.reshape(seqlen, width)
        start = pl.multiple_of(KV_HEADS * width + g * VALUE_DIM, VALUE_DIM)
        value = kv_all[:, :, pl.ds(start, VALUE_DIM)].reshape(seqlen, VALUE_DIM)
        for h in range(GROUP):
            column = pl.multiple_of((g * GROUP + h) * width, width)
            query = q_ref[:, pl.ds(column, width)].astype(jnp.float32)
            query = turn(query, cos_ref[...], sin_ref[...]).astype(bf16)
            query = query.astype(jnp.float32) * HEAD_DIM**-0.5
            maps = []
            for m in range(2):
                mine = (lane < HEAD_DIM) if m == 0 else (lane >= HEAD_DIM)
                part = jnp.where(mine, query, 0.0).astype(bf16)
                scores = lax.dot_general(
                    part, key, (((1,), (1,)), ((), ())), preferred_element_type=jnp.float32
                )
                scores = jnp.where(allowed, scores, -1e30)
                raised = jnp.exp(scores - jnp.max(scores, -1, keepdims=True))
                maps.append((raised, 1.0 / jnp.sum(raised, -1, keepdims=True)))
            lam = lam_ref[g * GROUP + h]
            weights = (
                maps[0][0] * maps[0][1] - maps[1][0] * (lam * maps[1][1])
            ).astype(bf16)
            found = jnp.dot(weights, value, preferred_element_type=jnp.float32)
            squares = jnp.mean(found * found, -1, keepdims=True)
            normed = found * lax.rsqrt(squares + norm_eps) * gain_ref[...] * output_scale
            heads_all[d, :, pl.ds(column, width)] = normed.astype(bf16)
        for copy in sends_of(g):
            copy.start()
        return carry

    lax.fori_loop(0, KV_HEADS // 2, one_group, 0)
    w_relay(1, 0)
    lax.fori_loop(KV_HEADS // 2, KV_HEADS, one_group, 0)
    w_relay(1, 1)

    forwards = []
    for g in range(KV_HEADS):
        copies = sends_of(g)
        for k in range(1, half):
            copies[k].wait_recv()
            part = heads_all.at[(x + half - k) % half * 2 + core, :, span(g)]
            forwards.append(
                send(part, part, mate_send.at[k, g], mate_recv.at[k, g], "dp", mate)
            )
            forwards[-1].start()
    for g in range(KV_HEADS):
        sends_of(g)[0].wait_recv()
    for copy in forwards:
        copy.wait_recv()

    heads = heads_all[...].reshape(count * rows, heads_all.shape[2])
    own = w_ref.shape[1]
    outs = []

    def project(index, places):
        slots = [at(place) for place in places]
        blocks = [w_all[slot] if index else w_ref[...] for slot in slots]
        if own % 128 == 0:
            both = jnp.concatenate(blocks, -1) if len(blocks) > 1 else blocks[0]
            both = jnp.dot(heads, both, preferred_element_type=jnp.float32).astype(bf16)
            results = [both[:, i * own : (i + 1) * own] for i in range(len(blocks))]
        else:
            results = [
                jnp.dot(heads, block, preferred_element_type=jnp.float32).astype(bf16)
                for block in blocks
            ]
        for i in range(len(slots)):
            built[index, i] = results[i].reshape(count, rows, own)
        for k in range(1, count):
            to = (d + k) % count
            for i in range(len(slots)):
                outs.append(
                    send(
                        built.at[index, i, to],
                        out_ref.at[slots[i], d],
                        out_send.at[index, i, k],
                        out_recv.at[index, i, k],
                        "dp",
                        to,
                    )
                )
                outs[-1].start()
        for i in range(len(slots)):
            out_ref[slots[i], d] = built[index, i, d]

    project(0, (pos,))
    for t in range(1, steps + 1):
        if t > 1:
            w_relay(t, 0)
            w_relay(t, 1)
        project(t, (pos - t, pos + t) if t < steps else (pos + t,))
    for copy in outs:
        copy.wait()
    for copies in list(kv_copies.values()) + list(w_copies.values()):
        for copy in copies:
            copy.wait_send()
    for g in range(KV_HEADS):
        for copy in sends_of(g):
            copy.wait_send()
    for copy in forwards:
        copy.wait_send()


def lay_kernel(in_ref, out_ref):
    own = in_ref.shape[2]
    for b in range(in_ref.shape[0]):
        out_ref[:, b * own : (b + 1) * own] = in_ref[b]


def shards(queries, keys, values, lambdas, value_gain, out_weight):
    rows = queries.shape[1]
    sp_count = lax.axis_size("sp")
    dp_count = lax.axis_size("dp")
    width = 2 * HEAD_DIM
    vmem = pl.BlockSpec(memory_space=pltpu.VMEM)
    bf16 = jnp.bfloat16
    positions = (lax.axis_index("sp") * rows + jnp.arange(rows)).astype(jnp.float32)
    cosine, sine = tables(positions)
    kv_width = 2 * KV_HEADS * width

    half = dp_count // 2
    steps = sp_count // 2
    depth, own = out_weight.shape
    dma = pltpu.SemaphoreType.DMA
    mixed = pl.pallas_call(
        functools.partial(layer_kernel, sp_count, dp_count),
        out_shape=jax.ShapeDtypeStruct((sp_count, dp_count, rows, own), bf16),
        in_specs=[pl.BlockSpec(memory_space=pltpu.SMEM)] + [vmem] * 7,
        out_specs=vmem,
        scratch_shapes=[
            pltpu.VMEM((rows, kv_width), bf16),
            pltpu.VMEM((sp_count, rows, kv_width), bf16),
            pltpu.VMEM((sp_count, depth, own), bf16),
            pltpu.VMEM((dp_count, rows, depth), bf16),
            pltpu.VMEM((steps + 1, 2, dp_count, rows, own), bf16),
            dma(()),
        ]
        + [dma((2, steps, 2))] * 4
        + [dma((half, KV_HEADS))] * 4
        + [dma((steps + 1, 2, dp_count))] * 2,
        compiler_params=pltpu.CompilerParams(
            collective_id=0, has_side_effects=True, vmem_limit_bytes=60 * 2**20
        ),
        name="layer",
    )(lambdas, queries[0], keys[0], values[0], cosine, sine, value_gain[None], out_weight)

    if own % 128 == 0:
        return pl.pallas_call(
            lay_kernel,
            out_shape=jax.ShapeDtypeStruct((rows, sp_count * dp_count * own), bf16),
            in_specs=[vmem],
            out_specs=vmem,
            name="lay",
        )(mixed.reshape(-1, rows, own))[None]
    return jnp.transpose(mixed, (2, 0, 1, 3)).reshape(1, rows, -1)


def solution(mesh):
    return jax.shard_map(
        shards,
        mesh=mesh,
        in_specs=(
            P("dp", "sp", None),
            P("dp", "sp", None),
            P("dp", "sp", None),
            P(),
            P(),
            P(None, ("sp", "dp")),
        ),
        out_specs=P("dp", "sp", None),
        check_vma=False,
    )
```

profile of v0, /device:TPU:0, one launch (start us, length us, event | category | flops | bytes accessed | tf_op | source)
XLA Modules:
  0.0 80.2 jit_solution(11524615417130204042)
XLA Ops:
  0.0 0.3 fusion
  0.3 0.8 %pad_maximum_fusion = (f32[128,128]{1,0:T(8,128)}, f32[128,128]{1,0:T(8,128)}) fusion(f32[128,32]{1,0:T(8,128)S(1)} %get-tuple-element.7, f32[128,32]{1,0:T(8,128)S(1)} %get-tuple-element.6, f32[128,32]{1,0:T(8,128)S(1)} %get-tuple-element.5), kind=kLoop, calls=%fused_computation.2 | loop fusion | flops 98304 | bytes 180224 | tf_op jit(solution)/shard_map/concatenate | solution.py:26
  1.2 76.6 %layer.1 = bf16[8,4,128,128]{3,2,1,0:T(8,128)(2,1)} custom-call(f32[16]{0:T(128)} %lam_ref.1, bf16[128,2048]{1,0:T(8,128)(2,1)} %bitcast.7, bf16[128,512]{1,0:T(8,128)(2,1)} %bitcast.8, bf16[128,512]{1,0:T(8,128)(2,1)} %bitcast.9, f32[128,128]{1,0:T(8,128)} %get-tuple-element.8.cos_ref, f32[128,128]{1,0:T(8,128)} %get-tuple-element.9.sin_ref, ...), custom_call_target="tpu_custom_call" | custom-call | tf_op jit(solution)/shard_map/layer/pallas_call | solution.py:309
  77.8 2.5 %lay.1 = bf16[128,4096]{1,0:T(8,128)(2,1)} custom-call(bf16[32,128,128]{2,1,0:T(8,128)(2,1)} %bitcast.6), custom_call_target="tpu_custom_call" | custom-call | tf_op jit(solution)/shard_map/lay/pallas_call | solution.py:332
  (2 shorter events, 0.0 us)
where the time goes:
time: 80.4 us; the launch traced here: 80.2 us
  Pallas kernels  79.1 us (98%)
  other arithmetic  1.15 us (1%)
    pallas_call x1, Pallas kernels, shards(): pl.pallas_call(functools.partial(layer_kernel, sp_count, dp_count), out_s...  76.6 us
    pallas_call x1, Pallas kernels, shards(): pl.pallas_call(lay_kernel, out_shape=jax.ShapeDtypeStruct((rows, sp_count...  2.47 us

commit v1 on v0

v1 whole, which is shorter than its diff:
```python
import functools

import jax
import jax.numpy as jnp
import numpy as np
from jax import lax
from jax.experimental import pallas as pl
from jax.experimental.pallas import tpu as pltpu
from jax.sharding import PartitionSpec as P

HEADS = 16
KV_HEADS = 4
HEAD_DIM = 64
VALUE_DIM = 128
GROUP = HEADS // KV_HEADS
WIDTH = 2 * HEAD_DIM

rope_base = 500000.0
output_scale = 0.8
norm_eps = 1e-05
MESH = pl.DeviceIdType.MESH


def tables(seqlen):
    freqs = rope_base ** (-np.arange(0, HEAD_DIM, 2, dtype=np.float64) / HEAD_DIM)
    angles = np.arange(seqlen, dtype=np.float64)[:, None] * freqs[None, :]
    cosine, sine = np.cos(angles).astype(np.float32), np.sin(angles).astype(np.float32)
    return np.concatenate([cosine] * 4, -1), np.concatenate([-sine, sine, -sine, sine], -1)


def turn(block, cosine, sine):
    half = HEAD_DIM // 2
    lane = lax.broadcasted_iota(jnp.int32, block.shape, 1)
    other = jnp.where(
        lane % HEAD_DIM < half,
        pltpu.roll(block, block.shape[1] - half, 1),
        pltpu.roll(block, half, 1),
    )
    return block * cosine + other * sine


def send(src, dst, send_sem, recv_sem, **device):
    return pltpu.make_async_remote_copy(
        src_ref=src,
        dst_ref=dst,
        send_sem=send_sem,
        recv_sem=recv_sem,
        device_id=device,
        device_id_type=MESH,
    )


def layer_kernel(
    sizes,
    lam_ref,
    q_ref,
    k_ref,
    v_ref,
    cos_ref,
    sin_ref,
    gain_ref,
    w_ref,
    out_ref,
    cos,
    sin,
    q_all,
    kv_own,
    kv_all,
    w_all,
    heads_all,
    built,
    local_sem,
    kvy_send,
    kvy_recv,
    q_send,
    q_recv,
    kvz_send,
    kvz_recv,
    w_send,
    w_recv,
    mate_send,
    mate_recv,
    h_send,
    h_recv,
    o_send,
    o_recv,
):
    bf16 = jnp.bfloat16
    Z, Y, X = sizes
    sp, dp = lax.axis_index("sp"), lax.axis_index("dp")
    z, y = sp // Y, sp % Y
    x, c = dp // 2, dp % 2
    rows = q_ref.shape[0]
    plane = Y * rows
    hpy = KV_HEADS // Y
    own_heads = hpy * GROUP
    span = own_heads * WIDTH
    own = w_ref.shape[1]
    peers = [(kx, ky) for kx in range(X) for ky in range(Y) if kx or ky]

    def place(kx, ky):
        return (x + kx) % X, (y + ky) % Y

    def in_plane(src, dst, sends, recvs, kx, ky):
        to_x, to_y = place(kx, ky)
        return send(src, dst, sends, recvs, sp=z * Y + to_y, dp=to_x * 2 + c)

    def along_z(src, dst, sends, recvs, up):
        to = jnp.minimum(z + 1, Z - 1) if up else jnp.maximum(z - 1, 0)
        return send(src, dst, sends, recvs, sp=to * Y + y)

    has_up, has_down = z < Z - 1, z > 0

    barrier = pltpu.get_barrier_semaphore()
    for kx, ky in peers:
        to_x, to_y = place(kx, ky)
        pl.semaphore_signal(
            barrier, inc=1, device_id={"sp": z * Y + to_y, "dp": to_x * 2 + c}, device_id_type=MESH
        )
    pl.semaphore_signal(barrier, inc=1, device_id={"dp": x * 2 + 1 - c}, device_id_type=MESH)

    @pl.when(has_up)
    def _():
        pl.semaphore_signal(barrier, inc=1, device_id={"sp": sp + Y}, device_id_type=MESH)

    @pl.when(has_down)
    def _():
        pl.semaphore_signal(barrier, inc=1, device_id={"sp": sp - Y}, device_id_type=MESH)

    start_row = pl.multiple_of(z * plane, plane)
    loads = [
        pltpu.make_async_copy(cos_ref.at[pl.ds(start_row, plane)], cos, local_sem.at[0]),
        pltpu.make_async_copy(sin_ref.at[pl.ds(start_row, plane)], sin, local_sem.at[1]),
        pltpu.make_async_copy(w_ref, w_all.at[z, c], local_sem.at[2]),
        pltpu.make_async_copy(
            q_ref.at[:, pl.ds(pl.multiple_of(y * span, span), span)], q_all.at[y], local_sem.at[3]
        ),
    ]
    for copy in loads:
        copy.start()
    loads[0].wait()
    loads[1].wait()
    mine = pl.ds(pl.multiple_of(y * rows, rows), rows)
    for g in range(KV_HEADS):
        cols = slice(g * WIDTH, (g + 1) * WIDTH)
        key = turn(k_ref[:, cols].astype(jnp.float32), cos[mine, :], sin[mine, :])
        kv_own[g, :, :WIDTH] = key.astype(bf16)
        kv_own[g, :, WIDTH:] = v_ref[:, cols]
    for h in range(hpy):
        kv_all[h, z, y] = kv_own[y * hpy + h]

    pl.semaphore_wait(
        barrier, X * Y + has_up.astype(jnp.int32) + has_down.astype(jnp.int32)
    )

    def kvy(h, k):
        to_y = (y + k) % Y
        return in_plane(
            kv_own.at[to_y * hpy + h], kv_all.at[h, z, y], kvy_send.at[k, h], kvy_recv.at[k, h], 0, k
        )

    def qy(h, k):
        to_y = (y + k) % Y
        piece = GROUP * WIDTH
        return in_plane(
            q_ref.at[:, pl.ds(pl.multiple_of((to_y * hpy + h) * piece, piece), piece)],
            q_all.at[y, :, pl.ds(h * piece, piece)],
            q_send.at[k, h],
            q_recv.at[k, h],
            0,
            k,
        )

    def kvz(h, k, k_y):
        at_y = (y - k_y + Y) % Y
        part = kv_all.at[h, jnp.maximum(z - k, 0), at_y]
        return along_z(part, part, kvz_send.at[h, k, k_y], kvz_recv.at[h, k, k_y], True)

    def kvz_wait(h, k, k_y):
        at_y = (y - k_y + Y) % Y
        part = kv_all.at[h, jnp.maximum(z - k, 0), at_y]
        along_z(part, part, kvz_send.at[h, k - 1, k_y], kvz_recv.at[h, k - 1, k_y], True).wait_recv()

    def w_move(up, k):
        piece = w_all.at[jnp.maximum(z - k, 0) if up else jnp.minimum(z + k, Z - 1), c]
        return along_z(piece, piece, w_send.at[int(up), k], w_recv.at[int(up), k], up)

    def w_mate(piece):
        part = w_all.at[piece, c]
        return send(part, part, mate_send.at[piece], mate_recv.at[piece], dp=x * 2 + 1 - c)

    def has_piece(up, k):
        return z >= k if up else z < Z - k

    def piece_of(up, k):
        return jnp.maximum(z - k, 0) if up else jnp.minimum(z + k, Z - 1)

    def w_relay(up, k):
        w_move(up, k - 1).wait_recv()
        w_mate(piece_of(up, k)).start()
        if k < Z - 1:

            @pl.when(has_up if up else has_down)
            def _():
                w_move(up, k).start()

    for h in range(hpy):
        for k in range(1, Y):
            kvy(h, k).start()

        @pl.when(has_up)
        def _():
            kvz(h, 0, 0).start()

    for h in range(hpy):
        for k in range(1, Y):
            qy(h, k).start()
    loads[2].wait()
    w_mate(z).start()

    @pl.when(has_down)
    def _():
        w_move(False, 0).start()

    for h in range(hpy):
        for k in range(1, Y):
            kvy(h, k).wait_recv()

            @pl.when(has_up)
            def _():
                kvz(h, 0, k).start()

    @pl.when(z == 0)
    def _():
        w_move(True, 0).start()

    def kv_relay(h, k):
        for k_y in range(Y):
            kvz_wait(h, k, k_y)
            if k < Z - 1:

                @pl.when(has_up)
                def _():
                    kvz(h, k, k_y).start()

    for k in range(1, Z):

        @pl.when(z >= k)
        def _():
            kv_relay(0, k)

    if hpy == 1:

        @pl.when(has_up & has_down)
        def _():
            w_move(True, 0).start()

    loads[3].wait()
    for k in range(1, Y):
        qy(0, k).wait_recv()

    lane = lax.broadcasted_iota(jnp.int32, (rows, WIDTH), 1)
    below = lax.broadcasted_iota(jnp.int32, (rows, plane), 1) - lax.broadcasted_iota(
        jnp.int32, (rows, plane), 0
    )
    blocks_per_h = GROUP * Y
    nt = (((1,), (1,)), ((), ()))

    def attend(depth, h, local_head, yb):
        query = q_all[yb, :, pl.ds(pl.multiple_of(local_head * WIDTH, WIDTH), WIDTH)]
        at = pl.ds(pl.multiple_of(yb * rows, rows), rows)
        query = turn(query.astype(jnp.float32), cos[at, :], sin[at, :]).astype(bf16)
        query = query.astype(jnp.float32) * HEAD_DIM**-0.5
        allowed = below <= yb * rows
        key = kv_all[h, : depth + 1, :, :, :WIDTH].reshape((depth + 1) * plane, WIDTH)
        value = kv_all[h, : depth + 1, :, :, WIDTH:].reshape((depth + 1) * plane, VALUE_DIM)
        maps = []
        for m in range(2):
            inside = (lane < HEAD_DIM) if m == 0 else (lane >= HEAD_DIM)
            part = jnp.where(inside, query, 0.0).astype(bf16)
            scores = lax.dot_general(part, key, nt, preferred_element_type=jnp.float32)
            last = jnp.where(allowed, scores[:, depth * plane :], -1e30)
            if depth:
                scores = jnp.concatenate([scores[:, : depth * plane], last], -1)
            else:
                scores = last
            raised = jnp.exp(scores - jnp.max(scores, -1, keepdims=True))
            maps.append((raised, jnp.sum(raised, -1, keepdims=True)))
        head = y * own_heads + local_head
        ratio = lam_ref[head] * maps[0][1] / maps[1][1]
        weights = (maps[0][0] - maps[1][0] * ratio).astype(bf16)
        found = jnp.dot(weights, value, preferred_element_type=jnp.float32) / maps[0][1]
        squares = jnp.mean(found * found, -1, keepdims=True)
        normed = found * lax.rsqrt(squares + norm_eps) * gain_ref[...] * output_scale
        at_row = pl.ds(pl.multiple_of(x * plane + yb * rows, rows), rows)
        heads_all[head, at_row, :] = normed.astype(bf16)

    def heads_send(local_head, index):
        kx, ky = peers[index]
        part = heads_all.at[
            y * own_heads + local_head, pl.ds(pl.multiple_of(x * plane, plane), plane)
        ]
        return in_plane(
            part, part, h_send.at[index, local_head], h_recv.at[index, local_head], kx, ky
        )

    def attend_step(i, carry):
        local_head, yb = i // Y, i % Y
        h = i // blocks_per_h
        for other in range(1, hpy):
            for k in range(1, Z):

                @pl.when((i == (other - 1) * blocks_per_h + k - 1) & (z >= k) & has_up)
                def _():
                    kv_relay(other, k)

                @pl.when((i == other * blocks_per_h) & (z >= k) & (z == Z - 1))
                def _():
                    kv_relay(other, k)

            @pl.when(i == other * blocks_per_h)
            def _():
                for k in range(1, Y):
                    qy(other, k).wait_recv()

        if hpy > 1:

            @pl.when((i == (hpy - 2) * blocks_per_h + Z - 1) & has_up & has_down)
            def _():
                w_move(True, 0).start()

        @pl.when((i == own_heads * Y * 5 // 8) & has_up)
        def _():
            w_relay(False, 1)

        for depth in range(Z):

            @pl.when(z == depth)
            def _():
                attend(depth, h, local_head, yb)

        @pl.when(yb == Y - 1)
        def _():
            for index in range(len(peers)):
                heads_send(local_head, index).start()

        return carry

    lax.fori_loop(0, own_heads * Y, attend_step, 0)

    @pl.when(has_down)
    def _():
        w_relay(True, 1)

    for local_head in range(own_heads):
        for index in range(len(peers)):
            heads_send(local_head, index).wait_recv()

    total = X * plane
    tall = min(total, 512)

    def out_send(piece, index):
        kx, ky = peers[index]
        to_x, to_y = place(kx, ky)
        src = built.at[piece, pl.ds(pl.multiple_of(to_x * plane + to_y * rows, rows), rows)]
        return in_plane(
            src, out_at(piece, x, y), o_send.at[piece, index], o_recv.at[piece, index], kx, ky
        )

    def out_at(piece, at_x, at_y):
        block = (piece * Y + at_y) * X + at_x
        if len(out_ref.shape) == 3:
            return out_ref.at[block]
        return out_ref.at[:, pl.ds(pl.multiple_of(block * 2 * own, 2 * own), 2 * own)]

    def project(piece):
        def one(step, carry):
            at = pl.ds(pl.multiple_of(step * tall, tall), tall)
            lhs = jnp.concatenate([heads_all[head, at, :] for head in range(HEADS)], -1)
            if own % 128 == 0:
                rhs = jnp.concatenate([w_all[piece, 0], w_all[piece, 1]], -1)
                built[piece, at, :] = jnp.dot(lhs, rhs, preferred_element_type=jnp.float32).astype(
                    bf16
                )
            else:
                for side in range(2):
                    built[piece, at, side * own : (side + 1) * own] = jnp.dot(
                        lhs, w_all[piece, side], preferred_element_type=jnp.float32
                    ).astype(bf16)
            return carry

        if total == tall:
            one(0, 0)
        else:
            lax.fori_loop(0, total // tall, one, 0)
        for index in range(len(peers)):
            out_send(piece, index).start()
        mine = pl.ds(pl.multiple_of(x * plane + y * rows, rows), rows)
        out_at(piece, x, y)[...] = built[piece, mine, :]

    w_mate(z).wait_recv()
    project(z)
    for k in range(1, Z):
        if k > 1:
            for up in (False, True):

                @pl.when(has_piece(up, k))
                def _():
                    w_relay(up, k)

        for up in (False, True):

            @pl.when(has_piece(up, k))
            def _():
                w_mate(piece_of(up, k)).wait_recv()
                project(piece_of(up, k))

    for piece in range(Z):
        for index in range(len(peers)):
            out_send(piece, index).wait()
    for h in range(hpy):
        for k in range(1, Y):
            kvy(h, k).wait_send()
            qy(h, k).wait_send()
        for k in range(Z - 1):

            @pl.when((z >= k) & has_up)
            def _():
                for k_y in range(Y):
                    kvz(h, k, k_y).wait_send()

    for k in range(Z - 1):

        @pl.when((z >= k) & has_up)
        def _():
            w_move(True, k).wait_send()

        @pl.when((z + k < Z) & has_down)
        def _():
            w_move(False, k).wait_send()

    for piece in range(Z):
        w_mate(piece).wait_send()
    for local_head in range(own_heads):
        for index in range(len(peers)):
            heads_send(local_head, index).wait_send()


def shards(queries, keys, values, lambdas, value_gain, out_weight):
    rows = queries.shape[1]
    sp_count = lax.axis_size("sp")
    dp_count = lax.axis_size("dp")
    X = Y = dp_count // 2
    Z = sp_count // Y
    hpy = KV_HEADS // Y
    own_heads = hpy * GROUP
    vmem = pl.BlockSpec(memory_space=pltpu.VMEM)
    far = pl.BlockSpec(memory_space=pl.ANY)
    bf16 = jnp.bfloat16
    cosine, sine = tables(sp_count * rows)
    depth, own = out_weight.shape
    plane = Y * rows
    blocks = Z * Y * X
    flat = 2 * own % 128 == 0
    shape = (rows, blocks * 2 * own) if flat else (blocks, rows, 2 * own)
    dma = pltpu.SemaphoreType.DMA
    mixed = pl.pallas_call(
        functools.partial(layer_kernel, (Z, Y, X)),
        out_shape=jax.ShapeDtypeStruct(shape, bf16),
        in_specs=[pl.BlockSpec(memory_space=pltpu.SMEM)] + [vmem] * 3 + [far] * 2 + [vmem, far],
        out_specs=vmem,
        scratch_shapes=[
            pltpu.VMEM((plane, WIDTH), jnp.float32),
            pltpu.VMEM((plane, WIDTH), jnp.float32),
            pltpu.VMEM((Y, rows, own_heads * WIDTH), bf16),
            pltpu.VMEM((KV_HEADS, rows, 2 * WIDTH), bf16),
            pltpu.VMEM((hpy, Z, Y, rows, 2 * WIDTH), bf16),
            pltpu.VMEM((Z, 2, depth, own), bf16),
            pltpu.VMEM((HEADS, X * plane, VALUE_DIM), bf16),
            pltpu.VMEM((Z, X * plane, 2 * own), bf16),
            dma((4,)),
        ]
        + [dma((Y, hpy))] * 4
        + [dma((hpy, Z, Y))] * 2
        + [dma((2, Z))] * 2
        + [dma((Z,))] * 2
        + [dma((X * Y - 1, own_heads))] * 2
        + [dma((Z, X * Y - 1))] * 2,
        compiler_params=pltpu.CompilerParams(
            collective_id=0, has_side_effects=True, vmem_limit_bytes=60 * 2**20
        ),
        name="layer",
    )(
        lambdas,
        queries[0],
        keys[0],
        values[0],
        jnp.asarray(cosine),
        jnp.asarray(sine),
        value_gain[None],
        out_weight,
    )
    if not flat:
        mixed = jnp.transpose(mixed, (1, 0, 2)).reshape(rows, -1)
    return mixed[None]


def solution(mesh):
    return jax.shard_map(
        shards,
        mesh=mesh,
        in_specs=(
            P("dp", "sp", None),
            P("dp", "sp", None),
            P("dp", "sp", None),
            P(),
            P(),
            P(None, ("sp", "dp")),
        ),
        out_specs=P("dp", "sp", None),
        check_vma=False,
    )
```

time: 80.4 us -> 66.6 us (0.83)
  the two profiles are of different devices: /device:TPU:0 before, /device:TPU:25 now
where the time goes in v1:
time: 66.6 us; the launch traced here: 66.4 us
  Pallas kernels  64.1 us (96%)
  local copies, waits for them, and re-layouts  2.29 us (3%)
    pallas_call x1, Pallas kernels, shards(): pl.pallas_call(functools.partial(layer_kernel, (Z, Y, X)), out_shape=jax....  64.1 us
    unnamed x1, local copies, waits for them, and re-layouts  2.29 us

profile of v1, /device:TPU:25, one launch (start us, length us, event | category | flops | bytes accessed | tf_op | source)
XLA Modules:
  0.0 66.4 jit_solution(1261875107102280463)
XLA Ops:
  0.0 64.1 %layer.1 = bf16[128,4096]{1,0:T(8,128)(2,1)} custom-call(f32[16]{0:T(128)} %lam_ref.1, bf16[128,2048]{1,0:T(8,128)(2,1)} %bitcast.6, bf16[128,512]{1,0:T(8,128)(2,1)} %bitcast.7, bf16[128,512]{1,0:T(8,128)(2,1)} %bitcast.8, f32[1024,128]{1,0:T(8,128)} %constant.4.clone.cos_ref, f32[1024,128]{1,0:T(8,128)} %constant.5.clone.sin_ref, f32[1,128]{1,0:T(1,128)} %bitcast.9, ...), custom_call_target="tpu_custom_call" | custom-call | tf_op jit(solution)/shard_map/layer/pallas_call | solution.py:467
  64.1 2.3 %copy.10 = bf16[1,128,4096]{2,1,0:T(8,128)(2,1)} copy(bf16[1,128,4096]{2,1,0:T(8,128)(2,1)} %bitcast.5) | data formatting | bytes 2097152

commit v2 on v1

--- a/solution.py
+++ b/solution.py
@@ -61,6 +61,8 @@
     gain_ref,
     w_ref,
     out_ref,
+    keys,
+    values,
     cos,
     sin,
     q_all,
@@ -111,13 +113,28 @@
 
     has_up, has_down = z < Z - 1, z > 0
 
+    start_row = pl.multiple_of(z * plane, plane)
+    loads = [
+        pltpu.make_async_copy(k_ref, keys, local_sem.at[0]),
+        pltpu.make_async_copy(cos_ref.at[pl.ds(start_row, plane)], cos, local_sem.at[1]),
+        pltpu.make_async_copy(sin_ref.at[pl.ds(start_row, plane)], sin, local_sem.at[2]),
+        pltpu.make_async_copy(v_ref, values, local_sem.at[3]),
+        pltpu.make_async_copy(
+            q_ref.at[:, pl.ds(pl.multiple_of(y * span, span), span)], q_all.at[y], local_sem.at[4]
+        ),
+        pltpu.make_async_copy(w_ref, w_all.at[z], local_sem.at[5]),
+    ]
+    for copy in loads:
+        copy.start()
+
     barrier = pltpu.get_barrier_semaphore()
-    for kx, ky in peers:
-        to_x, to_y = place(kx, ky)
-        pl.semaphore_signal(
-            barrier, inc=1, device_id={"sp": z * Y + to_y, "dp": to_x * 2 + c}, device_id_type=MESH
-        )
-    pl.semaphore_signal(barrier, inc=1, device_id={"dp": x * 2 + 1 - c}, device_id_type=MESH)
+    for kx in range(X):
+        for ky in range(Y):
+            to_x, to_y = place(kx, ky)
+            for kc in range(2):
+                if kx or ky or kc:
+                    to = {"sp": z * Y + to_y, "dp": to_x * 2 + (c + kc) % 2}
+                    pl.semaphore_signal(barrier, inc=1, device_id=to, device_id_type=MESH)
 
     @pl.when(has_up)
     def _():
@@ -127,30 +144,19 @@
     def _():
         pl.semaphore_signal(barrier, inc=1, device_id={"sp": sp - Y}, device_id_type=MESH)
 
-    start_row = pl.multiple_of(z * plane, plane)
-    loads = [
-        pltpu.make_async_copy(cos_ref.at[pl.ds(start_row, plane)], cos, local_sem.at[0]),
-        pltpu.make_async_copy(sin_ref.at[pl.ds(start_row, plane)], sin, local_sem.at[1]),
-        pltpu.make_async_copy(w_ref, w_all.at[z, c], local_sem.at[2]),
-        pltpu.make_async_copy(
-            q_ref.at[:, pl.ds(pl.multiple_of(y * span, span), span)], q_all.at[y], local_sem.at[3]
-        ),
-    ]
-    for copy in loads:
-        copy.start()
-    loads[0].wait()
-    loads[1].wait()
+    for copy in loads[:4]:
+        copy.wait()
     mine = pl.ds(pl.multiple_of(y * rows, rows), rows)
     for g in range(KV_HEADS):
         cols = slice(g * WIDTH, (g + 1) * WIDTH)
-        key = turn(k_ref[:, cols].astype(jnp.float32), cos[mine, :], sin[mine, :])
+        key = turn(keys[:, cols].astype(jnp.float32), cos[mine, :], sin[mine, :])
         kv_own[g, :, :WIDTH] = key.astype(bf16)
-        kv_own[g, :, WIDTH:] = v_ref[:, cols]
+        kv_own[g, :, WIDTH:] = values[:, cols]
     for h in range(hpy):
         kv_all[h, z, y] = kv_own[y * hpy + h]
 
     pl.semaphore_wait(
-        barrier, X * Y + has_up.astype(jnp.int32) + has_down.astype(jnp.int32)
+        barrier, 2 * X * Y - 1 + has_up.astype(jnp.int32) + has_down.astype(jnp.int32)
     )
 
     def kvy(h, k):
@@ -182,12 +188,8 @@
         along_z(part, part, kvz_send.at[h, k - 1, k_y], kvz_recv.at[h, k - 1, k_y], True).wait_recv()
 
     def w_move(up, k):
-        piece = w_all.at[jnp.maximum(z - k, 0) if up else jnp.minimum(z + k, Z - 1), c]
+        piece = w_all.at[piece_of(up, k)]
         return along_z(piece, piece, w_send.at[int(up), k], w_recv.at[int(up), k], up)
-
-    def w_mate(piece):
-        part = w_all.at[piece, c]
-        return send(part, part, mate_send.at[piece], mate_recv.at[piece], dp=x * 2 + 1 - c)
 
     def has_piece(up, k):
         return z >= k if up else z < Z - k
@@ -197,7 +199,6 @@
 
     def w_relay(up, k):
         w_move(up, k - 1).wait_recv()
-        w_mate(piece_of(up, k)).start()
         if k < Z - 1:
 
             @pl.when(has_up if up else has_down)
@@ -215,8 +216,7 @@
     for h in range(hpy):
         for k in range(1, Y):
             qy(h, k).start()
-    loads[2].wait()
-    w_mate(z).start()
+    loads[5].wait()
 
     @pl.when(has_down)
     def _():
@@ -255,7 +255,7 @@
         def _():
             w_move(True, 0).start()
 
-    loads[3].wait()
+    loads[4].wait()
     for k in range(1, Y):
         qy(0, k).wait_recv()
 
@@ -292,17 +292,24 @@
         found = jnp.dot(weights, value, preferred_element_type=jnp.float32) / maps[0][1]
         squares = jnp.mean(found * found, -1, keepdims=True)
         normed = found * lax.rsqrt(squares + norm_eps) * gain_ref[...] * output_scale
-        at_row = pl.ds(pl.multiple_of(x * plane + yb * rows, rows), rows)
+        at_row = pl.ds(pl.multiple_of(dp * plane + yb * rows, rows), rows)
         heads_all[head, at_row, :] = normed.astype(bf16)
 
     def heads_send(local_head, index):
         kx, ky = peers[index]
         part = heads_all.at[
-            y * own_heads + local_head, pl.ds(pl.multiple_of(x * plane, plane), plane)
+            y * own_heads + local_head, pl.ds(pl.multiple_of(dp * plane, plane), plane)
         ]
         return in_plane(
-            part, part, h_send.at[index, local_head], h_recv.at[index, local_head], kx, ky
+            part, part, h_send.at[index], h_recv.at[index, local_head], kx, ky
         )
+
+    def heads_mate(local_head, index):
+        kx, ky = peers[index] if index < len(peers) else (0, 0)
+        from_x, from_y = (x - kx + X) % X, (y - ky + Y) % Y
+        at = pl.ds(pl.multiple_of((from_x * 2 + c) * plane, plane), plane)
+        part = heads_all.at[from_y * own_heads + local_head, at]
+        return send(part, part, mate_send.at[index], mate_recv.at[index], dp=x * 2 + 1 - c)
 
     def attend_step(i, carry):
         local_head, yb = i // Y, i % Y
@@ -343,107 +350,123 @@
         def _():
             for index in range(len(peers)):
                 heads_send(local_head, index).start()
+            heads_mate(local_head, len(peers)).start()
 
         return carry
 
     lax.fori_loop(0, own_heads * Y, attend_step, 0)
 
-    @pl.when(has_down)
-    def _():
-        w_relay(True, 1)
-
+    def relay_if(up, k, extra=True):
+        if k < Z:
+
+            @pl.when(has_piece(up, k) & extra)
+            def _():
+                w_relay(up, k)
+
+    all_chunks = heads_all.at[pl.ds(0, own_heads), pl.ds(0, plane)]
+
+    def chunks_done(sem):
+        pltpu.make_async_copy(all_chunks, all_chunks, sem).wait()
+
+    relay_if(True, 1)
+    relay_if(False, 2)
     for local_head in range(own_heads):
         for index in range(len(peers)):
             heads_send(local_head, index).wait_recv()
-
-    total = X * plane
-    tall = min(total, 512)
-
-    def out_send(piece, index):
-        kx, ky = peers[index]
-        to_x, to_y = place(kx, ky)
-        src = built.at[piece, pl.ds(pl.multiple_of(to_x * plane + to_y * rows, rows), rows)]
-        return in_plane(
-            src, out_at(piece, x, y), o_send.at[piece, index], o_recv.at[piece, index], kx, ky
-        )
-
-    def out_at(piece, at_x, at_y):
-        block = (piece * Y + at_y) * X + at_x
+            heads_mate(local_head, index).start()
+    relay_if(True, 2, has_up)
+    for index in range(len(peers) + 1):
+        chunks_done(mate_recv.at[index])
+
+    def out_at(piece, at_x, at_y, at_c):
+        block = ((piece * Y + at_y) * X + at_x) * 2 + at_c
         if len(out_ref.shape) == 3:
             return out_ref.at[block]
-        return out_ref.at[:, pl.ds(pl.multiple_of(block * 2 * own, 2 * own), 2 * own)]
+        return out_ref.at[:, pl.ds(pl.multiple_of(block * own, own), own)]
+
+    def out_send(piece, kx, ky, kc):
+        to_x, to_y = place(kx, ky)
+        to_c = (c + kc) % 2
+        start = pl.multiple_of((to_x * 2 + to_c) * plane + to_y * rows, rows)
+        return send(
+            built.at[piece, pl.ds(start, rows)],
+            out_at(piece, x, y, c),
+            o_send,
+            o_recv,
+            sp=z * Y + to_y,
+            dp=to_x * 2 + to_c,
+        )
 
     def project(piece):
         def one(step, carry):
-            at = pl.ds(pl.multiple_of(step * tall, tall), tall)
+            kx = (step + 1) % X
+            tall = 2 * plane
+            at = pl.ds(pl.multiple_of((x + kx) % X * tall, tall), tall)
             lhs = jnp.concatenate([heads_all[head, at, :] for head in range(HEADS)], -1)
-            if own % 128 == 0:
-                rhs = jnp.concatenate([w_all[piece, 0], w_all[piece, 1]], -1)
-                built[piece, at, :] = jnp.dot(lhs, rhs, preferred_element_type=jnp.float32).astype(
-                    bf16
-                )
-            else:
-                for side in range(2):
-                    built[piece, at, side * own : (side + 1) * own] = jnp.dot(
-                        lhs, w_all[piece, side], preferred_element_type=jnp.float32
-                    ).astype(bf16)
+            found = jnp.dot(lhs, w_all[piece], preferred_element_type=jnp.float32)
+            built[piece, at, :] = found.astype(bf16)
+            for ky in reversed(range(Y)):
+                for kc in reversed(range(2)):
+                    if ky or kc:
+                        out_send(piece, kx, ky, kc).start()
+                    else:
+
+                        @pl.when(kx > 0)
+                        def _():
+                            out_send(piece, kx, 0, 0).start()
+
             return carry
 
-        if total == tall:
-            one(0, 0)
-        else:
-            lax.fori_loop(0, total // tall, one, 0)
+        lax.fori_loop(0, X, one, 0)
+        mine = pl.ds(pl.multiple_of(dp * plane + y * rows, rows), rows)
+        out_at(piece, x, y, c)[...] = built[piece, mine, :]
+
+    def finish_sends():
+        for h in range(hpy):
+            for k in range(1, Y):
+                kvy(h, k).wait_send()
+                qy(h, k).wait_send()
+            for k in range(Z - 1):
+
+                @pl.when((z >= k) & has_up)
+                def _():
+                    for k_y in range(Y):
+                        kvz(h, k, k_y).wait_send()
+
         for index in range(len(peers)):
-            out_send(piece, index).start()
-        mine = pl.ds(pl.multiple_of(x * plane + y * rows, rows), rows)
-        out_at(piece, x, y)[...] = built[piece, mine, :]
-
-    w_mate(z).wait_recv()
+            chunks_done(h_send.at[index])
+        for index in range(len(peers) + 1):
+            chunks_done(mate_send.at[index])
+        for k in range(Z - 1):
+
+            @pl.when((z + k < Z) & has_down)
+            def _():
+                w_move(False, k).wait_send()
+
     project(z)
     for k in range(1, Z):
-        if k > 1:
-            for up in (False, True):
-
-                @pl.when(has_piece(up, k))
-                def _():
-                    w_relay(up, k)
-
+        if k > 2:
+            relay_if(False, k)
+        if k == Z - 1:
+            finish_sends()
+        if k == 2:
+            relay_if(True, k, ~has_up)
+        elif k > 2:
+            relay_if(True, k)
         for up in (False, True):
 
             @pl.when(has_piece(up, k))
             def _():
-                w_mate(piece_of(up, k)).wait_recv()
                 project(piece_of(up, k))
 
-    for piece in range(Z):
-        for index in range(len(peers)):
-            out_send(piece, index).wait()
-    for h in range(hpy):
-        for k in range(1, Y):
-            kvy(h, k).wait_send()
-            qy(h, k).wait_send()
-        for k in range(Z - 1):
-
-            @pl.when((z >= k) & has_up)
-            def _():
-                for k_y in range(Y):
-                    kvz(h, k, k_y).wait_send()
-
+    others = built.at[:, pl.ds(0, (2 * X * Y - 1) * rows)]
+    pltpu.make_async_copy(others, others, o_recv).wait()
+    pltpu.make_async_copy(others, others, o_send).wait()
     for k in range(Z - 1):
 
         @pl.when((z >= k) & has_up)
         def _():
             w_move(True, k).wait_send()
-
-        @pl.when((z + k < Z) & has_down)
-        def _():
-            w_move(False, k).wait_send()
-
-    for piece in range(Z):
-        w_mate(piece).wait_send()
-    for local_head in range(own_heads):
-        for index in range(len(peers)):
-            heads_send(local_head, index).wait_send()
 
 
 def shards(queries, keys, values, lambdas, value_gain, out_weight):
@@ -455,50 +478,52 @@
     hpy = KV_HEADS // Y
     own_heads = hpy * GROUP
     vmem = pl.BlockSpec(memory_space=pltpu.VMEM)
-    far = pl.BlockSpec(memory_space=pl.ANY)
+    far = pl.BlockSpec(memory_space=pltpu.HBM)
     bf16 = jnp.bfloat16
     cosine, sine = tables(sp_count * rows)
     depth, own = out_weight.shape
     plane = Y * rows
-    blocks = Z * Y * X
-    flat = 2 * own % 128 == 0
-    shape = (rows, blocks * 2 * own) if flat else (blocks, rows, 2 * own)
+    blocks = Z * Y * X * 2
+    flat = own % 128 == 0
+    shape = (rows, blocks * own) if flat else (blocks, rows, own)
     dma = pltpu.SemaphoreType.DMA
     mixed = pl.pallas_call(
         functools.partial(layer_kernel, (Z, Y, X)),
-        out_shape=jax.ShapeDtypeStruct(shape, bf16),
-        in_specs=[pl.BlockSpec(memory_space=pltpu.SMEM)] + [vmem] * 3 + [far] * 2 + [vmem, far],
+        out_shape=pltpu.VMEM(shape, bf16),
+        in_specs=[pl.BlockSpec(memory_space=pltpu.SMEM)] + [far] * 5 + [vmem, far],
         out_specs=vmem,
         scratch_shapes=[
+            pltpu.VMEM((rows, KV_HEADS * WIDTH), bf16),
+            pltpu.VMEM((rows, KV_HEADS * VALUE_DIM), bf16),
             pltpu.VMEM((plane, WIDTH), jnp.float32),
             pltpu.VMEM((plane, WIDTH), jnp.float32),
             pltpu.VMEM((Y, rows, own_heads * WIDTH), bf16),
             pltpu.VMEM((KV_HEADS, rows, 2 * WIDTH), bf16),
             pltpu.VMEM((hpy, Z, Y, rows, 2 * WIDTH), bf16),
-            pltpu.VMEM((Z, 2, depth, own), bf16),
-            pltpu.VMEM((HEADS, X * plane, VALUE_DIM), bf16),
-            pltpu.VMEM((Z, X * plane, 2 * own), bf16),
-            dma((4,)),
+            pltpu.VMEM((Z, depth, own), bf16),
+            pltpu.VMEM((HEADS, 2 * X * plane, VALUE_DIM), bf16),
+            pltpu.VMEM((Z, 2 * X * plane, own), bf16),
+            dma((6,)),
         ]
         + [dma((Y, hpy))] * 4
         + [dma((hpy, Z, Y))] * 2
         + [dma((2, Z))] * 2
-        + [dma((Z,))] * 2
-        + [dma((X * Y - 1, own_heads))] * 2
-        + [dma((Z, X * Y - 1))] * 2,
+        + [dma((X * Y,))] * 2
+        + [dma((X * Y - 1,)), dma((X * Y - 1, own_heads))]
+        + [dma(())] * 2,
         compiler_params=pltpu.CompilerParams(
-            collective_id=0, has_side_effects=True, vmem_limit_bytes=60 * 2**20
+            collective_id=0, has_side_effects=True, vmem_limit_bytes=40 * 2**20
         ),
         name="layer",
     )(
-        lambdas,
-        queries[0],
-        keys[0],
-        values[0],
-        jnp.asarray(cosine),
-        jnp.asarray(sine),
-        value_gain[None],
-        out_weight,
+        pltpu.with_memory_space_constraint(lambdas, pltpu.HBM),
+        pltpu.with_memory_space_constraint(queries[0], pltpu.HBM),
+        pltpu.with_memory_space_constraint(keys[0], pltpu.HBM),
+        pltpu.with_memory_space_constraint(values[0], pltpu.HBM),
+        pltpu.with_memory_space_constraint(jnp.asarray(cosine), pltpu.HBM),
+        pltpu.with_memory_space_constraint(jnp.asarray(sine), pltpu.HBM),
+        pltpu.with_memory_space_constraint(value_gain[None], pltpu.HBM),
+        pltpu.with_memory_space_constraint(out_weight, pltpu.HBM),
     )
     if not flat:
         mixed = jnp.transpose(mixed, (1, 0, 2)).reshape(rows, -1)

time: 66.6 us -> 62.6 us (0.940)
  Pallas kernels: 64.1 us -> 61.1 us
  local copies, waits for them, and re-layouts: 2.29 us -> 0.97 us
    pallas_call x1, Pallas kernels: 64.1 us -> 61.1 us  [shards(): pl.pallas_call(functools.partial(layer_kernel, (Z, Y, X)), out_shape=pltp...]
    unnamed x1, local copies, waits for them, and re-layouts: 2.29 us -> 0.97 us
where the time goes in v2:
time: 62.6 us; the launch traced here: 62.1 us
  Pallas kernels  61.1 us (98%)
  local copies, waits for them, and re-layouts  0.97 us (2%)
    pallas_call x1, Pallas kernels, shards(): pl.pallas_call(functools.partial(layer_kernel, (Z, Y, X)), out_shape=pltp...  61.1 us

profile of v2, /device:TPU:25, one launch (start us, length us, event | category | flops | bytes accessed | tf_op | source)
XLA Modules:
  0.0 62.1 jit_solution(5099260148680739794)
XLA Ops:
  0.0 61.1 %layer.1 = bf16[128,4096]{1,0:T(8,128)(2,1)S(1)} custom-call(f32[16]{0:T(128)} %lam_ref.1, bf16[128,2048]{1,0:T(8,128)(2,1)} %bitcast.6, bf16[128,512]{1,0:T(8,128)(2,1)} %bitcast.7, bf16[128,512]{1,0:T(8,128)(2,1)} %bitcast.8, f32[1024,128]{1,0:T(8,128)} %constant.4.clone.cos_ref, f32[1024,128]{1,0:T(8,128)} %constant.5.clone.sin_ref, f32[1,128]{1,0:T(1,128)} %bitcast.9, ...), custom_call_target="tpu_custom_call" | custom-call | tf_op jit(solution)/shard_map/layer/pallas_call | solution.py:490
  61.1 1.0 %copy.10 = bf16[1,128,4096]{2,1,0:T(8,128)(2,1)} copy(bf16[1,128,4096]{2,1,0:T(8,128)(2,1)S(1)} %bitcast.5) | data formatting | bytes 2097152

commit v3 on v2

--- a/solution.py
+++ b/solution.py
@@ -70,12 +70,19 @@
     kv_all,
     w_all,
     heads_all,
+    heads_up,
     built,
     local_sem,
     kvy_send,
     kvy_recv,
     q_send,
     q_recv,
+    kvt_send,
+    kvt_recv,
+    qt_send,
+    qt_recv,
+    hz_send,
+    hz_recv,
     kvz_send,
     kvz_recv,
     w_send,
@@ -112,15 +119,18 @@
         return send(src, dst, sends, recvs, sp=to * Y + y)
 
     has_up, has_down = z < Z - 1, z > 0
-
-    start_row = pl.multiple_of(z * plane, plane)
+    top, helper, kv_up = z == Z - 1, z == Z - 2, z < Z - 2
+    parts = 4
+
+    first = jnp.minimum(z, Z - 2)
+    start_row = pl.multiple_of(first * plane, plane)
     loads = [
         pltpu.make_async_copy(k_ref, keys, local_sem.at[0]),
-        pltpu.make_async_copy(cos_ref.at[pl.ds(start_row, plane)], cos, local_sem.at[1]),
-        pltpu.make_async_copy(sin_ref.at[pl.ds(start_row, plane)], sin, local_sem.at[2]),
+        pltpu.make_async_copy(cos_ref.at[pl.ds(start_row, 2 * plane)], cos, local_sem.at[1]),
+        pltpu.make_async_copy(sin_ref.at[pl.ds(start_row, 2 * plane)], sin, local_sem.at[2]),
         pltpu.make_async_copy(v_ref, values, local_sem.at[3]),
         pltpu.make_async_copy(
-            q_ref.at[:, pl.ds(pl.multiple_of(y * span, span), span)], q_all.at[y], local_sem.at[4]
+            q_ref.at[:, pl.ds(pl.multiple_of(y * span, span), span)], q_all.at[0, y], local_sem.at[4]
         ),
         pltpu.make_async_copy(w_ref, w_all.at[z], local_sem.at[5]),
     ]
@@ -146,7 +156,7 @@
 
     for copy in loads[:4]:
         copy.wait()
-    mine = pl.ds(pl.multiple_of(y * rows, rows), rows)
+    mine = pl.ds(pl.multiple_of((z - first) * plane + y * rows, rows), rows)
     for g in range(KV_HEADS):
         cols = slice(g * WIDTH, (g + 1) * WIDTH)
         key = turn(keys[:, cols].astype(jnp.float32), cos[mine, :], sin[mine, :])
@@ -155,14 +165,13 @@
     for h in range(hpy):
         kv_all[h, z, y] = kv_own[y * hpy + h]
 
-    pl.semaphore_wait(
-        barrier, 2 * X * Y - 1 + has_up.astype(jnp.int32) + has_down.astype(jnp.int32)
-    )
+    near = has_up.astype(jnp.int32) + has_down.astype(jnp.int32)
+    pl.semaphore_wait(barrier, 2 * X * Y - 1 + near)
 
     def kvy(h, k):
         to_y = (y + k) % Y
         return in_plane(
-            kv_own.at[to_y * hpy + h], kv_all.at[h, z, y], kvy_send.at[k, h], kvy_recv.at[k, h], 0, k
+            kv_own.at[to_y * hpy + h], kv_all.at[h, z, y], kvy_send, kvy_recv.at[k - 1, h], 0, k
         )
 
     def qy(h, k):
@@ -170,26 +179,53 @@
         piece = GROUP * WIDTH
         return in_plane(
             q_ref.at[:, pl.ds(pl.multiple_of((to_y * hpy + h) * piece, piece), piece)],
-            q_all.at[y, :, pl.ds(h * piece, piece)],
-            q_send.at[k, h],
-            q_recv.at[k, h],
+            q_all.at[0, y, :, pl.ds(h * piece, piece)],
+            q_send,
+            q_recv.at[k - 1, h],
             0,
             k,
         )
 
+    def kvt(h, k):
+        part = kv_all.at[h, Z - 1, (y - k + Y) % Y]
+        return send(part, part, kvt_send, kvt_recv.at[h], sp=(Z - 2) * Y + y)
+
+    def qt(h, k):
+        piece = GROUP * WIDTH
+        at_y = (y - k + Y) % Y
+        cols = pl.ds(h * piece, piece)
+        return send(
+            q_all.at[0, at_y, :, cols],
+            q_all.at[1, at_y, :, cols],
+            qt_send,
+            qt_recv.at[h],
+            sp=(Z - 2) * Y + y,
+        )
+
+    def hz(local_head):
+        return send(
+            heads_up.at[local_head],
+            heads_part(local_head, 0, 0),
+            hz_send,
+            hz_recv.at[local_head],
+            sp=(Z - 1) * Y + y,
+        )
+
     def kvz(h, k, k_y):
         at_y = (y - k_y + Y) % Y
         part = kv_all.at[h, jnp.maximum(z - k, 0), at_y]
-        return along_z(part, part, kvz_send.at[h, k, k_y], kvz_recv.at[h, k, k_y], True)
+        return along_z(part, part, kvz_send, kvz_recv.at[h, k, k_y], True)
 
     def kvz_wait(h, k, k_y):
         at_y = (y - k_y + Y) % Y
         part = kv_all.at[h, jnp.maximum(z - k, 0), at_y]
-        along_z(part, part, kvz_send.at[h, k - 1, k_y], kvz_recv.at[h, k - 1, k_y], True).wait_recv()
-
-    def w_move(up, k):
-        piece = w_all.at[piece_of(up, k)]
-        return along_z(piece, piece, w_send.at[int(up), k], w_recv.at[int(up), k], up)
+        along_z(part, part, kvz_send, kvz_recv.at[h, k - 1, k_y], True).wait_recv()
+
+    def w_move(up, k, part):
+        cut = w_all.shape[1] // parts
+        piece = w_all.at[piece_of(up, k), pl.ds(part * cut, cut)]
+        side = int(up)
+        return along_z(piece, piece, w_send.at[side], w_recv.at[side, k, part], up)
 
     def has_piece(up, k):
         return z >= k if up else z < Z - k
@@ -197,81 +233,132 @@
     def piece_of(up, k):
         return jnp.maximum(z - k, 0) if up else jnp.minimum(z + k, Z - 1)
 
-    def w_relay(up, k):
-        w_move(up, k - 1).wait_recv()
+    def w_relay(up, k, part):
+        w_move(up, k - 1, part).wait_recv()
         if k < Z - 1:
 
             @pl.when(has_up if up else has_down)
             def _():
-                w_move(up, k).start()
+                w_move(up, k, part).start()
+
+    def w_own(up, some=range(4)):
+        for part in some:
+            w_move(up, 0, part).start()
+
+    middle = has_up & has_down
 
     for h in range(hpy):
         for k in range(1, Y):
             kvy(h, k).start()
 
-        @pl.when(has_up)
+        @pl.when(kv_up if h == 0 else z == 0)
         def _():
             kvz(h, 0, 0).start()
 
-    for h in range(hpy):
         for k in range(1, Y):
             qy(h, k).start()
-    loads[5].wait()
+
+    @pl.when(helper)
+    def _():
+        loads[5].wait()
+        w_own(True)
+
+    for k in range(1, Y):
+        kvy(0, k).wait_recv()
+
+        @pl.when(kv_up)
+        def _():
+            kvz(0, 0, k).start()
+
+    @pl.when(top)
+    def _():
+        loads[4].wait()
+        for h in range(hpy):
+            for k in range(Y):
+                if k and h:
+                    kvy(h, k).wait_recv()
+                if k:
+                    qy(h, k).wait_recv()
+                kvt(h, k).start()
+                qt(h, k).start()
+
+    @pl.when(~helper)
+    def _():
+        loads[5].wait()
 
     @pl.when(has_down)
     def _():
-        w_move(False, 0).start()
-
-    for h in range(hpy):
+        w_own(False)
+
+    def late_kv(h):
         for k in range(1, Y):
             kvy(h, k).wait_recv()
 
-            @pl.when(has_up)
-            def _():
+    @pl.when(z == 0)
+    def _():
+        for h in range(1, hpy):
+            late_kv(h)
+            for k in range(1, Y):
                 kvz(h, 0, k).start()
 
-    @pl.when(z == 0)
-    def _():
-        w_move(True, 0).start()
+    if Z > 2:
+
+        @pl.when(z == 0)
+        def _():
+            w_own(True)
 
     def kv_relay(h, k):
         for k_y in range(Y):
             kvz_wait(h, k, k_y)
-            if k < Z - 1:
-
-                @pl.when(has_up)
+            if k < Z - 2:
+
+                @pl.when(kv_up)
                 def _():
                     kvz(h, k, k_y).start()
 
-    for k in range(1, Z):
-
-        @pl.when(z >= k)
+    for k in range(1, Z - 1):
+
+        @pl.when((z >= k) & has_up)
         def _():
             kv_relay(0, k)
 
-    if hpy == 1:
-
-        @pl.when(has_up & has_down)
-        def _():
-            w_move(True, 0).start()
-
-    loads[4].wait()
-    for k in range(1, Y):
-        qy(0, k).wait_recv()
-
-    lane = lax.broadcasted_iota(jnp.int32, (rows, WIDTH), 1)
-    below = lax.broadcasted_iota(jnp.int32, (rows, plane), 1) - lax.broadcasted_iota(
-        jnp.int32, (rows, plane), 0
+    @pl.when(kv_up & has_down)
+    def _():
+        w_own(True, range(2))
+        for h in range(1, hpy):
+            late_kv(h)
+            for k in range(Y):
+                kvz(h, 0, k).start()
+        if hpy == 1:
+            w_own(True, range(2, 4))
+
+    @pl.when(has_up)
+    def _():
+        loads[4].wait()
+        for k in range(1, Y):
+            qy(0, k).wait_recv()
+
+    def done(ref, sem):
+        pltpu.make_async_copy(ref, ref, sem).wait()
+
+    def take_top(h):
+        done(kv_all.at[h, Z - 1], kvt_recv.at[h])
+        done(q_all.at[1, :, :, pl.ds(h * GROUP * WIDTH, GROUP * WIDTH)], qt_recv.at[h])
+
+    lane = lax.broadcasted_iota(jnp.int32, (plane, WIDTH), 1)
+    allowed = lax.broadcasted_iota(jnp.int32, (plane, plane), 1) <= lax.broadcasted_iota(
+        jnp.int32, (plane, plane), 0
     )
-    blocks_per_h = GROUP * Y
     nt = (((1,), (1,)), ((), ()))
-
-    def attend(depth, h, local_head, yb):
-        query = q_all[yb, :, pl.ds(pl.multiple_of(local_head * WIDTH, WIDTH), WIDTH)]
-        at = pl.ds(pl.multiple_of(yb * rows, rows), rows)
-        query = turn(query.astype(jnp.float32), cos[at, :], sin[at, :]).astype(bf16)
+    lag = 2
+    direct = own_heads - 2
+
+    def attend(depth, h, local_head, above=0):
+        at = pl.ds(pl.multiple_of(local_head * WIDTH, WIDTH), WIDTH)
+        query = q_all[above, :, :, at].reshape(plane, WIDTH)
+        table = pl.ds(above * plane, plane)
+        query = turn(query.astype(jnp.float32), cos[table, :], sin[table, :]).astype(bf16)
         query = query.astype(jnp.float32) * HEAD_DIM**-0.5
-        allowed = below <= yb * rows
         key = kv_all[h, : depth + 1, :, :, :WIDTH].reshape((depth + 1) * plane, WIDTH)
         value = kv_all[h, : depth + 1, :, :, WIDTH:].reshape((depth + 1) * plane, VALUE_DIM)
         maps = []
@@ -292,89 +379,162 @@
         found = jnp.dot(weights, value, preferred_element_type=jnp.float32) / maps[0][1]
         squares = jnp.mean(found * found, -1, keepdims=True)
         normed = found * lax.rsqrt(squares + norm_eps) * gain_ref[...] * output_scale
-        at_row = pl.ds(pl.multiple_of(dp * plane + yb * rows, rows), rows)
-        heads_all[head, at_row, :] = normed.astype(bf16)
-
-    def heads_send(local_head, index):
-        kx, ky = peers[index]
-        part = heads_all.at[
-            y * own_heads + local_head, pl.ds(pl.multiple_of(dp * plane, plane), plane)
-        ]
-        return in_plane(
-            part, part, h_send.at[index], h_recv.at[index, local_head], kx, ky
-        )
-
-    def heads_mate(local_head, index):
-        kx, ky = peers[index] if index < len(peers) else (0, 0)
+        if above:
+            heads_up[local_head] = normed.astype(bf16)
+        else:
+            at_row = pl.ds(pl.multiple_of(dp * plane, plane), plane)
+            heads_all[head, at_row, :] = normed.astype(bf16)
+
+    def heads_part(local_head, kx, ky):
         from_x, from_y = (x - kx + X) % X, (y - ky + Y) % Y
         at = pl.ds(pl.multiple_of((from_x * 2 + c) * plane, plane), plane)
-        part = heads_all.at[from_y * own_heads + local_head, at]
+        return heads_all.at[from_y * own_heads + local_head, at]
+
+    def heads_send(local_head, to, start=(0, 0)):
+        index = peers.index(to)
+        part = heads_part(local_head, *start)
+        hop = (to[0] - start[0], to[1] - start[1])
+        return in_plane(part, part, h_send.at[index], h_recv.at[index, local_head], *hop)
+
+    straight = [peer for peer in peers if not (peer[0] and peer[1])]
+    corners = [peer for peer in peers if peer[0] and peer[1]]
+
+    def heads_relay(local_head):
+        for peer in straight:
+            heads_send(local_head, peer).wait_recv()
+            heads_mate(local_head, peer).start()
+            parity = 0 if peer[0] else 1
+
+            @pl.when((local_head % 2 == parity) & (local_head < direct))
+            def _():
+                for corner in corners:
+                    if corner[parity] == peer[parity]:
+                        heads_send(local_head, corner, peer).start()
+
+    def heads_mate(local_head, peer):
+        index = peers.index(peer) if peer in peers else len(peers)
+        part = heads_part(local_head, *peer)
         return send(part, part, mate_send.at[index], mate_recv.at[index], dp=x * 2 + 1 - c)
 
     def attend_step(i, carry):
-        local_head, yb = i // Y, i % Y
-        h = i // blocks_per_h
+        h = i // GROUP
         for other in range(1, hpy):
-            for k in range(1, Z):
-
-                @pl.when((i == (other - 1) * blocks_per_h + k - 1) & (z >= k) & has_up)
+            for k in range(1, Z - 1):
+
+                @pl.when((i == (other - 1) * GROUP + k - 1) & (z >= k) & kv_up)
                 def _():
                     kv_relay(other, k)
 
-                @pl.when((i == other * blocks_per_h) & (z >= k) & (z == Z - 1))
-                def _():
-                    kv_relay(other, k)
-
-            @pl.when(i == other * blocks_per_h)
+            @pl.when((i == other * GROUP) & has_up)
             def _():
                 for k in range(1, Y):
                     qy(other, k).wait_recv()
 
         if hpy > 1:
 
-            @pl.when((i == (hpy - 2) * blocks_per_h + Z - 1) & has_up & has_down)
-            def _():
-                w_move(True, 0).start()
-
-        @pl.when((i == own_heads * Y * 5 // 8) & has_up)
-        def _():
-            w_relay(False, 1)
-
-        for depth in range(Z):
+            @pl.when((i == (hpy - 2) * GROUP + Z - 3) & kv_up & has_down)
+            def _():
+                w_own(True, range(2, 4))
+
+        for up, k, part, step, where in in_loop:
+
+            @pl.when((i == step) & where)
+            def _():
+                w_relay(up, k, part)
+
+        for depth in range(Z - 1):
 
             @pl.when(z == depth)
             def _():
-                attend(depth, h, local_head, yb)
-
-        @pl.when(yb == Y - 1)
-        def _():
-            for index in range(len(peers)):
-                heads_send(local_head, index).start()
-            heads_mate(local_head, len(peers)).start()
+                attend(depth, h, i)
+
+        @pl.when(top)
+        def _():
+            hz(i).wait_recv()
+
+        for peer in straight:
+            heads_send(i, peer).start()
+        heads_mate(i, (0, 0)).start()
+
+        @pl.when(i >= direct)
+        def _():
+            for peer in corners:
+                heads_send(i, peer).start()
+
+        @pl.when(i >= lag)
+        def _():
+            heads_relay(i - lag)
+
+        @pl.when(helper & (i == GROUP - 1))
+        def _():
+            for other in range(hpy):
+                if other:
+                    late_kv(other)
+                    for k in range(1, Z - 1):
+
+                        @pl.when(z >= k)
+                        def _():
+                            kv_relay(other, k)
+
+                for up, k, part, step, where in in_loop:
+                    if step == slots + other:
+                        w_relay(up, k, part)
+                take_top(other)
+
+                def above_step(j, carry):
+                    attend(Z - 1, other, j, 1)
+                    hz(j).start()
+                    return carry
+
+                lax.fori_loop(other * GROUP, (other + 1) * GROUP, above_step, 0)
 
         return carry
 
-    lax.fori_loop(0, own_heads * Y, attend_step, 0)
-
-    def relay_if(up, k, extra=True):
-        if k < Z:
-
-            @pl.when(has_piece(up, k) & extra)
-            def _():
-                w_relay(up, k)
+    slots = own_heads
+    in_loop = []
+    if slots >= 8 and Z > 3:
+        for part in range(parts):
+            in_loop.append((True, 1, part, 3 + part, middle & ~helper))
+            in_loop.append((False, 1, part, 2 + part, middle & ~helper))
+            in_loop.append((True, 1, part, (3, slots + 1, 4, 5)[part], helper))
+        for part in range(2):
+            in_loop.append((False, 1, part, 5 + 2 * part, helper))
+        in_loop.append((True, 2, 0, 7, helper))
+    lax.fori_loop(0, own_heads, attend_step, 0)
+
+    def relay_rest(up, k, part):
+        done = z < 0
+        for up_, k_, part_, _, where in in_loop:
+            if (up_, k_, part_) == (up, k, part):
+                done = done | where
+        return ~done & has_piece(up, k)
+
+    def relay_if(up, k, where, some=range(4)):
+        if k >= Z:
+            return
+        for part in some:
+
+            @pl.when(relay_rest(up, k, part) & where)
+            def _():
+                w_relay(up, k, part)
 
     all_chunks = heads_all.at[pl.ds(0, own_heads), pl.ds(0, plane)]
 
     def chunks_done(sem):
         pltpu.make_async_copy(all_chunks, all_chunks, sem).wait()
 
-    relay_if(True, 1)
-    relay_if(False, 2)
+    relay_if(True, 1, middle)
+    relay_if(True, 2, helper & has_down, range(2))
+    for local_head in range(own_heads - lag, own_heads):
+        heads_relay(jnp.int32(local_head))
+    relay_if(False, 1, middle)
+    relay_if(True, 2, helper & has_down, range(2, 3))
     for local_head in range(own_heads):
-        for index in range(len(peers)):
-            heads_send(local_head, index).wait_recv()
-            heads_mate(local_head, index).start()
-    relay_if(True, 2, has_up)
+        for peer in corners:
+            heads_send(local_head, peer).wait_recv()
+            heads_mate(local_head, peer).start()
+        if local_head == own_heads // 2:
+            relay_if(True, 2, helper & has_down, range(3, 4))
     for index in range(len(peers) + 1):
         chunks_done(mate_recv.at[index])
 
@@ -422,51 +582,65 @@
         out_at(piece, x, y, c)[...] = built[piece, mine, :]
 
     def finish_sends():
-        for h in range(hpy):
-            for k in range(1, Y):
-                kvy(h, k).wait_send()
-                qy(h, k).wait_send()
-            for k in range(Z - 1):
-
-                @pl.when((z >= k) & has_up)
-                def _():
-                    for k_y in range(Y):
-                        kvz(h, k, k_y).wait_send()
+        if Y > 1:
+            done(kv_own.at[pl.ds(0, hpy * (Y - 1))], kvy_send)
+            done(q_all.at[0, pl.ds(0, Y - 1)], q_send)
+
+        @pl.when(top)
+        def _():
+            done(kv_own, kvt_send)
+            done(q_all.at[0], qt_send)
+
+        @pl.when(helper)
+        def _():
+            done(heads_up, hz_send)
+
+        for depth in range(Z - 2):
+
+            @pl.when(z == depth)
+            def _():
+                done(kv_all.at[:, pl.ds(0, depth + 1)], kvz_send)
 
         for index in range(len(peers)):
             chunks_done(h_send.at[index])
         for index in range(len(peers) + 1):
             chunks_done(mate_send.at[index])
-        for k in range(Z - 1):
-
-            @pl.when((z + k < Z) & has_down)
-            def _():
-                w_move(False, k).wait_send()
-
+        for depth in range(1, Z):
+
+            @pl.when(z == depth)
+            def _():
+                done(w_all.at[pl.ds(0, Z - depth)], w_send.at[0])
+
+    inner = middle & ~helper
+
+    def project_if(up, k):
+        @pl.when(has_piece(up, k))
+        def _():
+            project(piece_of(up, k))
+
+    relay_if(False, 2, inner, range(1))
     project(z)
+    relay_if(False, 2, inner, range(1, 2))
     for k in range(1, Z):
-        if k > 2:
-            relay_if(False, k)
         if k == Z - 1:
             finish_sends()
-        if k == 2:
-            relay_if(True, k, ~has_up)
-        elif k > 2:
-            relay_if(True, k)
-        for up in (False, True):
-
-            @pl.when(has_piece(up, k))
-            def _():
-                project(piece_of(up, k))
+        relay_if(False, k, ~middle if k < 3 else z >= 0)
+        relay_if(True, k, ~middle if k == 1 else ~(helper & has_down) if k == 2 else z >= 0)
+        project_if(False, k)
+        if k == 1:
+            relay_if(False, 2, inner, range(2, 3))
+        project_if(True, k)
+        if k == 1:
+            relay_if(False, 2, inner, range(3, 4))
 
     others = built.at[:, pl.ds(0, (2 * X * Y - 1) * rows)]
     pltpu.make_async_copy(others, others, o_recv).wait()
     pltpu.make_async_copy(others, others, o_send).wait()
-    for k in range(Z - 1):
-
-        @pl.when((z >= k) & has_up)
-        def _():
-            w_move(True, k).wait_send()
+    for depth in range(Z - 1):
+
+        @pl.when(z == depth)
+        def _():
+            done(w_all.at[pl.ds(0, depth + 1)], w_send.at[1])
 
 
 def shards(queries, keys, values, lambdas, value_gain, out_weight):
@@ -495,19 +669,22 @@
         scratch_shapes=[
             pltpu.VMEM((rows, KV_HEADS * WIDTH), bf16),
             pltpu.VMEM((rows, KV_HEADS * VALUE_DIM), bf16),
-            pltpu.VMEM((plane, WIDTH), jnp.float32),
-            pltpu.VMEM((plane, WIDTH), jnp.float32),
-            pltpu.VMEM((Y, rows, own_heads * WIDTH), bf16),
+            pltpu.VMEM((2 * plane, WIDTH), jnp.float32),
+            pltpu.VMEM((2 * plane, WIDTH), jnp.float32),
+            pltpu.VMEM((2, Y, rows, own_heads * WIDTH), bf16),
             pltpu.VMEM((KV_HEADS, rows, 2 * WIDTH), bf16),
             pltpu.VMEM((hpy, Z, Y, rows, 2 * WIDTH), bf16),
             pltpu.VMEM((Z, depth, own), bf16),
             pltpu.VMEM((HEADS, 2 * X * plane, VALUE_DIM), bf16),
+            pltpu.VMEM((own_heads, plane, VALUE_DIM), bf16),
             pltpu.VMEM((Z, 2 * X * plane, own), bf16),
             dma((6,)),
         ]
-        + [dma((Y, hpy))] * 4
-        + [dma((hpy, Z, Y))] * 2
-        + [dma((2, Z))] * 2
+        + [dma(()), dma((Y - 1, hpy))] * 2
+        + [dma(()), dma((hpy,))] * 2
+        + [dma(()), dma((own_heads,))]
+        + [dma(()), dma((hpy, max(Z - 2, 1), Y))]
+        + [dma((2,)), dma((2, Z - 1, 4))]
         + [dma((X * Y,))] * 2
         + [dma((X * Y - 1,)), dma((X * Y - 1, own_heads))]
         + [dma(())] * 2,

time: 62.6 us -> 61.5 us (0.982)
  the two profiles are of different devices: /device:TPU:25 before, /device:TPU:0 now
where the time goes in v3:
time: 61.5 us; the launch traced here: 61.4 us
  Pallas kernels  60.4 us (98%)
  local copies, waits for them, and re-layouts  0.97 us (2%)
    pallas_call x1, Pallas kernels, shards(): pl.pallas_call(functools.partial(layer_kernel, (Z, Y, X)), out_shape=pltp...  60.4 us

profile of v3, /device:TPU:0, one launch (start us, length us, event | category | flops | bytes accessed | tf_op | source)
XLA Modules:
  0.0 61.4 jit_solution(17385716612532093184)
XLA Ops:
  0.0 60.4 %layer.1 = bf16[128,4096]{1,0:T(8,128)(2,1)S(1)} custom-call(f32[16]{0:T(128)} %lam_ref.1, bf16[128,2048]{1,0:T(8,128)(2,1)} %bitcast.6, bf16[128,512]{1,0:T(8,128)(2,1)} %bitcast.7, bf16[128,512]{1,0:T(8,128)(2,1)} %bitcast.8, f32[1024,128]{1,0:T(8,128)} %constant.4.clone.cos_ref, f32[1024,128]{1,0:T(8,128)} %constant.5.clone.sin_ref, f32[1,128]{1,0:T(1,128)} %bitcast.9, ...), custom_call_target="tpu_custom_call" | custom-call | tf_op jit(solution)/shard_map/layer/pallas_call | solution.py:664
  60.4 1.0 %copy.10 = bf16[1,128,4096]{2,1,0:T(8,128)(2,1)} copy(bf16[1,128,4096]{2,1,0:T(8,128)(2,1)S(1)} %bitcast.5) | data formatting | bytes 2097152

commit v4 on v3

--- a/solution.py
+++ b/solution.py
@@ -121,6 +121,7 @@
     has_up, has_down = z < Z - 1, z > 0
     top, helper, kv_up = z == Z - 1, z == Z - 2, z < Z - 2
     parts = 4
+    moved = max(1, hpy // 2)
 
     first = jnp.minimum(z, Z - 2)
     start_row = pl.multiple_of(first * plane, plane)
@@ -251,7 +252,7 @@
         for k in range(1, Y):
             kvy(h, k).start()
 
-        @pl.when(kv_up if h == 0 else z == 0)
+        @pl.when(kv_up if h == 0 else kv_up & (z == 0))
         def _():
             kvz(h, 0, 0).start()
 
@@ -261,7 +262,7 @@
     @pl.when(helper)
     def _():
         loads[5].wait()
-        w_own(True)
+        w_own(True, range(3) if moved < hpy else range(4))
 
     for k in range(1, Y):
         kvy(0, k).wait_recv()
@@ -273,7 +274,7 @@
     @pl.when(top)
     def _():
         loads[4].wait()
-        for h in range(hpy):
+        for h in range(moved):
             for k in range(Y):
                 if k and h:
                     kvy(h, k).wait_recv()
@@ -294,7 +295,7 @@
         for k in range(1, Y):
             kvy(h, k).wait_recv()
 
-    @pl.when(z == 0)
+    @pl.when(kv_up & (z == 0))
     def _():
         for h in range(1, hpy):
             late_kv(h)
@@ -303,16 +304,16 @@
 
     if Z > 2:
 
-        @pl.when(z == 0)
+        @pl.when(kv_up & (z == 0))
         def _():
             w_own(True)
 
     def kv_relay(h, k):
         for k_y in range(Y):
             kvz_wait(h, k, k_y)
-            if k < Z - 2:
-
-                @pl.when(kv_up)
+            if k < (Z - 1 if h >= moved else Z - 2):
+
+                @pl.when(has_up if h >= moved else kv_up)
                 def _():
                     kvz(h, k, k_y).start()
 
@@ -324,13 +325,20 @@
 
     @pl.when(kv_up & has_down)
     def _():
-        w_own(True, range(2))
         for h in range(1, hpy):
             late_kv(h)
             for k in range(Y):
                 kvz(h, 0, k).start()
         if hpy == 1:
-            w_own(True, range(2, 4))
+            w_own(True)
+
+    @pl.when(helper)
+    def _():
+        for h in range(1, hpy):
+            late_kv(h)
+            if h >= moved:
+                for k in range(Y):
+                    kvz(h, 0, k).start()
 
     @pl.when(has_up)
     def _():
@@ -353,10 +361,10 @@
     lag = 2
     direct = own_heads - 2
 
-    def attend(depth, h, local_head, above=0):
+    def attend(depth, h, local_head, above=0, table=0):
         at = pl.ds(pl.multiple_of(local_head * WIDTH, WIDTH), WIDTH)
         query = q_all[above, :, :, at].reshape(plane, WIDTH)
-        table = pl.ds(above * plane, plane)
+        table = pl.ds(table * plane, plane)
         query = turn(query.astype(jnp.float32), cos[table, :], sin[table, :]).astype(bf16)
         query = query.astype(jnp.float32) * HEAD_DIM**-0.5
         key = kv_all[h, : depth + 1, :, :, :WIDTH].reshape((depth + 1) * plane, WIDTH)
@@ -399,13 +407,19 @@
     straight = [peer for peer in peers if not (peer[0] and peer[1])]
     corners = [peer for peer in peers if peer[0] and peer[1]]
 
-    def heads_relay(local_head):
+    kept = (hpy - moved) * GROUP
+
+    def order(position):
+        return jnp.where(top, (position + moved * GROUP) % own_heads, position)
+
+    def heads_relay(position):
+        local_head = order(position)
         for peer in straight:
             heads_send(local_head, peer).wait_recv()
             heads_mate(local_head, peer).start()
             parity = 0 if peer[0] else 1
 
-            @pl.when((local_head % 2 == parity) & (local_head < direct))
+            @pl.when((position % 2 == parity) & (position < direct))
             def _():
                 for corner in corners:
                     if corner[parity] == peer[parity]:
@@ -417,7 +431,8 @@
         return send(part, part, mate_send.at[index], mate_recv.at[index], dp=x * 2 + 1 - c)
 
     def attend_step(i, carry):
-        h = i // GROUP
+        head = order(i)
+        h = head // GROUP
         for other in range(1, hpy):
             for k in range(1, Z - 1):
 
@@ -425,6 +440,22 @@
                 def _():
                     kv_relay(other, k)
 
+                if other >= moved:
+
+                    @pl.when((i == min(k + 1, GROUP - 1)) & (z >= k) & helper)
+                    def _():
+                        kv_relay(other, k)
+
+            if other >= moved:
+
+                @pl.when((i == (other - moved) * GROUP) & top)
+                def _():
+                    late_kv(other)
+                    for k in range(1, Z):
+                        kv_relay(other, k)
+                    for k in range(1, Y):
+                        qy(other, k).wait_recv()
+
             @pl.when((i == other * GROUP) & has_up)
             def _():
                 for k in range(1, Y):
@@ -434,7 +465,13 @@
 
             @pl.when((i == (hpy - 2) * GROUP + Z - 3) & kv_up & has_down)
             def _():
-                w_own(True, range(2, 4))
+                w_own(True)
+
+            if moved < hpy:
+
+                @pl.when((i == GROUP) & helper)
+                def _():
+                    w_own(True, range(3, 4))
 
         for up, k, part, step, where in in_loop:
 
@@ -446,20 +483,26 @@
 
             @pl.when(z == depth)
             def _():
-                attend(depth, h, i)
-
-        @pl.when(top)
-        def _():
-            hz(i).wait_recv()
+                attend(depth, h, head)
+
+        @pl.when(top & (i >= kept))
+        def _():
+            hz(head).wait_recv()
+
+        if moved < hpy:
+
+            @pl.when(top & (i < kept))
+            def _():
+                attend(Z - 1, h, head, 0, 1)
 
         for peer in straight:
-            heads_send(i, peer).start()
-        heads_mate(i, (0, 0)).start()
+            heads_send(head, peer).start()
+        heads_mate(head, (0, 0)).start()
 
         @pl.when(i >= direct)
         def _():
             for peer in corners:
-                heads_send(i, peer).start()
+                heads_send(head, peer).start()
 
         @pl.when(i >= lag)
         def _():
@@ -467,9 +510,8 @@
 
         @pl.when(helper & (i == GROUP - 1))
         def _():
-            for other in range(hpy):
+            for other in range(moved):
                 if other:
-                    late_kv(other)
                     for k in range(1, Z - 1):
 
                         @pl.when(z >= k)
@@ -482,7 +524,7 @@
                 take_top(other)
 
                 def above_step(j, carry):
-                    attend(Z - 1, other, j, 1)
+                    attend(Z - 1, other, j, 1, 1)
                     hz(j).start()
                     return carry
 
@@ -496,10 +538,10 @@
         for part in range(parts):
             in_loop.append((True, 1, part, 3 + part, middle & ~helper))
             in_loop.append((False, 1, part, 2 + part, middle & ~helper))
-            in_loop.append((True, 1, part, (3, slots + 1, 4, 5)[part], helper))
+            if part < 3:
+                in_loop.append((True, 1, part, (4, 5, 7)[part], helper))
         for part in range(2):
-            in_loop.append((False, 1, part, 5 + 2 * part, helper))
-        in_loop.append((True, 2, 0, 7, helper))
+            in_loop.append((False, 1, part, 6 + part, helper))
     lax.fori_loop(0, own_heads, attend_step, 0)
 
     def relay_rest(up, k, part):
@@ -588,8 +630,8 @@
 
         @pl.when(top)
         def _():
-            done(kv_own, kvt_send)
-            done(q_all.at[0], qt_send)
+            done(kv_own.at[pl.ds(0, moved * Y)], kvt_send)
+            done(q_all.at[0, :, :, pl.ds(0, moved * GROUP * WIDTH)], qt_send)
 
         @pl.when(helper)
         def _():
@@ -600,6 +642,12 @@
             @pl.when(z == depth)
             def _():
                 done(kv_all.at[:, pl.ds(0, depth + 1)], kvz_send)
+
+        if moved < hpy:
+
+            @pl.when(helper)
+            def _():
+                done(kv_all.at[pl.ds(moved, hpy - moved), pl.ds(0, Z - 1)], kvz_send)
 
         for index in range(len(peers)):
             chunks_done(h_send.at[index])
@@ -651,6 +699,7 @@
     Z = sp_count // Y
     hpy = KV_HEADS // Y
     own_heads = hpy * GROUP
+    moved = max(1, hpy // 2)
     vmem = pl.BlockSpec(memory_space=pltpu.VMEM)
     far = pl.BlockSpec(memory_space=pltpu.HBM)
     bf16 = jnp.bfloat16
@@ -676,14 +725,14 @@
             pltpu.VMEM((hpy, Z, Y, rows, 2 * WIDTH), bf16),
             pltpu.VMEM((Z, depth, own), bf16),
             pltpu.VMEM((HEADS, 2 * X * plane, VALUE_DIM), bf16),
-            pltpu.VMEM((own_heads, plane, VALUE_DIM), bf16),
+            pltpu.VMEM((moved * GROUP, plane, VALUE_DIM), bf16),
             pltpu.VMEM((Z, 2 * X * plane, own), bf16),
             dma((6,)),
         ]
         + [dma(()), dma((Y - 1, hpy))] * 2
-        + [dma(()), dma((hpy,))] * 2
-        + [dma(()), dma((own_heads,))]
-        + [dma(()), dma((hpy, max(Z - 2, 1), Y))]
+        + [dma(()), dma((moved,))] * 2
+        + [dma(()), dma((moved * GROUP,))]
+        + [dma(()), dma((hpy, Z - 1, Y))]
         + [dma((2,)), dma((2, Z - 1, 4))]
         + [dma((X * Y,))] * 2
         + [dma((X * Y - 1,)), dma((X * Y - 1, own_heads))]

time: 61.5 us -> 59.9 us (0.974)
  the two profiles are of different devices: /device:TPU:0 before, /device:TPU:25 now
where the time goes in v4:
time: 59.9 us; the launch traced here: 59.7 us
  Pallas kernels  58.7 us (98%)
  local copies, waits for them, and re-layouts  0.97 us (2%)
    pallas_call x1, Pallas kernels, shards(): pl.pallas_call(functools.partial(layer_kernel, (Z, Y, X)), out_shape=pltp...  58.7 us

profile of v4, /device:TPU:25, one launch (start us, length us, event | category | flops | bytes accessed | tf_op | source)
XLA Modules:
  0.0 59.7 jit_solution(6654256518324699921)
XLA Ops:
  0.0 58.7 %layer.1 = bf16[128,4096]{1,0:T(8,128)(2,1)S(1)} custom-call(f32[16]{0:T(128)} %lam_ref.1, bf16[128,2048]{1,0:T(8,128)(2,1)} %bitcast.6, bf16[128,512]{1,0:T(8,128)(2,1)} %bitcast.7, bf16[128,512]{1,0:T(8,128)(2,1)} %bitcast.8, f32[1024,128]{1,0:T(8,128)} %constant.4.clone.cos_ref, f32[1024,128]{1,0:T(8,128)} %constant.5.clone.sin_ref, f32[1,128]{1,0:T(1,128)} %bitcast.9, ...), custom_call_target="tpu_custom_call" | custom-call | tf_op jit(solution)/shard_map/layer/pallas_call | solution.py:713
  58.7 1.0 %copy.10 = bf16[1,128,4096]{2,1,0:T(8,128)(2,1)} copy(bf16[1,128,4096]{2,1,0:T(8,128)(2,1)S(1)} %bitcast.5) | data formatting | bytes 2097152
